TPU v7x, 32 devices: a whole 2x2x4 slice. The times are simulated.
32 devices in a mesh: rep: 2 (over x), fs: 8 (over z, y), tp: 2 (over core).
Axes of the slice: x: 2, y: 2, z: 4, core: 2. Of those that a mesh axis runs over, the one named last changes fastest.
Arguments:
- stream_in: bfloat16 [16, 768, 2048], P(('rep', 'fs'), None, 'tp'), may hold values from -6 to 6
- mix_gain: float32 [2048], replicated, may hold values from 0.1 to 1.9
- lin_weight: bfloat16 [2048, 2048], P('fs', 'tp'), may hold values from -0.125 to 0.125
- branch_weight: bfloat16 [2048, 2048], P('fs', 'tp'), may hold values from -0.125 to 0.125
- lin_taps: float32 [4, 2048], P(None, 'tp'), may hold values from -3 to 3
- rate_blocks: bfloat16 [16, 128, 128], P('tp'), may hold values from -0.5 to 0.5
- admit_blocks: bfloat16 [16, 128, 128], P('tp'), may hold values from -0.5 to 0.5
- decay_logit: float32 [2048], P('tp'), may hold values from 3.5 to 9
- mix_out_gain: float32 [2048], P('tp'), may hold values from 0.1 to 1.9
- out_weight: bfloat16 [2048, 2048], P('tp', 'fs'), may hold values from -0.125 to 0.125
- ffn_gain: float32 [2048], replicated, may hold values from 0.1 to 1.9
- gate_weight: bfloat16 [2048, 2816], P('fs', 'tp'), may hold values from -0.125 to 0.125
- up_weight: bfloat16 [2048, 2816], P('fs', 'tp'), may hold values from -0.125 to 0.125
- gate_taps: float32 [3, 2816], P(None, 'tp'), may hold values from -3 to 3
- up_taps: float32 [3, 2816], P(None, 'tp'), may hold values from -3 to 3
- down_weight: bfloat16 [2816, 2048], P('tp', 'fs'), may hold values from -0.109375 to 0.109375
Outputs:
- stream_out: bfloat16 [16, 768, 2048], P(('rep', 'fs'), None, 'tp')
All inputs are finite; a program needn't handle non-finite values.
Results may differ from a plain program's by a relative error of at most 0.018.
Values may be sent and summed in bfloat16 or wider, within the bound.
A program may use at most 128 MiB of HBM per device.

v0:
```python
import jax
import jax.numpy as jnp
from jax import lax
from jax.sharding import PartitionSpec as P

EPS = 1e-06
GATE_SCALE = 8.0


def norm_rows(values, scales):
    mean_sq = jnp.mean(values * values, axis=-1, keepdims=True)
    return values * lax.rsqrt(mean_sq + EPS) * scales


def causal_filter(values, kernel):
    kernel_len = kernel.shape[0]
    seq_len = values.shape[0]
    padded = jnp.pad(values, ((kernel_len - 1, 0), (0, 0)))
    summed = padded[0:seq_len] * kernel[0]
    for offset in range(1, kernel_len):
        summed = summed + padded[offset : offset + seq_len] * kernel[offset]
    return summed


def chain_combine(earlier, later):
    return (earlier[0] * later[0], later[0] * earlier[1] + later[1])


def pair_folder(source, pieces):
    return (
        jnp.dot(source, pieces[0], preferred_element_type=jnp.float32),
        jnp.dot(source, pieces[1], preferred_element_type=jnp.float32),
    )


def local(
    stream_in,
    mix_gain,
    lin_weight,
    branch_weight,
    lin_taps,
    rate_blocks,
    admit_blocks,
    decay_logit,
    mix_out_gain,
    out_weight,
    ffn_gain,
    gate_weight,
    up_weight,
    gate_taps,
    up_taps,
    down_weight,
):
    own_rows = stream_in[0]
    length = own_rows.shape[0]
    full_rows = lax.all_gather(own_rows, "tp", axis=1, tiled=True)
    normed = norm_rows(full_rows.astype(jnp.float32), mix_gain).astype(jnp.bfloat16)
    linear, branch = pair_folder(
        normed,
        (
            lax.all_gather(lin_weight, "fs", axis=0, tiled=True),
            lax.all_gather(branch_weight, "fs", axis=0, tiled=True),
        ),
    )
    linear = linear.astype(jnp.bfloat16)
    branch = branch.astype(jnp.bfloat16)
    filtered = causal_filter(linear.astype(jnp.float32), lin_taps)
    block_count = rate_blocks.shape[0]
    block_width = rate_blocks.shape[1]
    blocks = filtered.astype(jnp.bfloat16).reshape(length, block_count, block_width)
    rate_gate = jax.nn.sigmoid(
        jnp.einsum("lbi,bij->lbj", blocks, rate_blocks, preferred_element_type=jnp.float32).reshape(
            length, -1
        )
    )
    admitted = jax.nn.sigmoid(
        jnp.einsum(
            "lbi,bij->lbj", blocks, admit_blocks, preferred_element_type=jnp.float32
        ).reshape(length, -1)
    )
    log_decay = -GATE_SCALE * rate_gate * jax.nn.softplus(-decay_logit)
    decay = jnp.exp(log_decay)
    driven = jnp.sqrt(-jnp.expm1(2.0 * log_decay)) * admitted * filtered
    _, states = lax.associative_scan(chain_combine, (decay, driven), axis=0)
    gated = (states * jax.nn.gelu(branch.astype(jnp.float32))).reshape(
        length, block_count, block_width
    )
    gated = gated * lax.rsqrt(jnp.mean(gated * gated, axis=-1, keepdims=True) + EPS)
    mixed = (gated.reshape(length, -1) * mix_out_gain).astype(jnp.bfloat16)
    mix_partial = jnp.dot(
        mixed,
        lax.all_gather(out_weight, "fs", axis=1, tiled=True),
        preferred_element_type=jnp.float32,
    )
    my_share = lax.psum_scatter(
        mix_partial.astype(jnp.bfloat16), "tp", scatter_dimension=1, tiled=True
    ).astype(jnp.float32)
    middle_own = (own_rows.astype(jnp.float32) + my_share).astype(jnp.bfloat16)
    middle_full = lax.all_gather(middle_own, "tp", axis=1, tiled=True)
    normed2 = norm_rows(middle_full.astype(jnp.float32), ffn_gain).astype(jnp.bfloat16)
    gate_pre, up_pre = pair_folder(
        normed2,
        (
            lax.all_gather(gate_weight, "fs", axis=0, tiled=True),
            lax.all_gather(up_weight, "fs", axis=0, tiled=True),
        ),
    )
    gate_pre = gate_pre.astype(jnp.bfloat16)
    up_pre = up_pre.astype(jnp.bfloat16)
    gate_conv = causal_filter(gate_pre.astype(jnp.float32), gate_taps)
    up_conv = causal_filter(up_pre.astype(jnp.float32), up_taps)
    hidden = (jax.nn.silu(gate_conv) * up_conv).astype(jnp.bfloat16)
    down_partial = jnp.dot(
        hidden,
        lax.all_gather(down_weight, "fs", axis=1, tiled=True),
        preferred_element_type=jnp.float32,
    )
    down_share = lax.psum_scatter(
        down_partial.astype(jnp.bfloat16), "tp", scatter_dimension=1, tiled=True
    ).astype(jnp.float32)
    result = (middle_own.astype(jnp.float32) + down_share).astype(jnp.bfloat16)
    return result[None]


def solution(mesh):
    placed = (
        P(("rep", "fs"), None, "tp"),
        P(),
        P("fs", "tp"),
        P("fs", "tp"),
        P(None, "tp"),
        P("tp", None, None),
        P("tp", None, None),
        P("tp"),
        P("tp"),
        P("tp", "fs"),
        P(),
        P("fs", "tp"),
        P("fs", "tp"),
        P(None, "tp"),
        P(None, "tp"),
        P("tp", "fs"),
    )
    return jax.shard_map(
        local, mesh=mesh, in_specs=placed, out_specs=P(("rep", "fs"), None, "tp"), check_vma=False
    )
```

profile of v0, /device:TPU:0, one launch (start us, length us, event | category | flops | bytes accessed | tf_op | source)
XLA Modules:
  0.0 664.1 jit_solution(280949965899593257)
XLA Ops:
  9.4 14.3 %all-gather.24.cloned.1.call-done = bf16[1,768,2048]{2,1,0:T(8,128)(2,1)} async-done(((bf16[1,768,1024]{2,1,0:T(8,128)(2,1)}), bf16[1,768,2048]{2,1,0:T(8,128)(2,1)}) %all-gather.24.cloned.1.call-update) | async-done | bytes 3145744 | tf_op jit(solution)/shard_map/all_gather | solution.py:56
  26.5 73.4 %all-gather.10.cloned.1.call-done = bf16[2048,1024]{1,0:T(8,128)(2,1)} async-done(((bf16[256,1024]{1,0:T(8,128)(2,1)}), bf16[2048,1024]{1,0:T(8,128)(2,1)}) %all-gather.10.cloned.1.call-update) | async-done | bytes 4194320 | tf_op jit(solution)/shard_map/all_gather | solution.py:61
  99.9 5.3 fusion.18
  116.6 7.7 %multiply_exponential_fusion = (f32[768,1024]{1,0:T(8,128)}, f32[768,1024]{1,0:T(8,128)S(1)}) fusion(f32[768,1024]{1,0:T(8,128)} %copy.40, f32[1024]{0:T(1024)S(1)} %fusion.40, f32[768,1024]{1,0:T(8,128)} %get-tuple-element.14, f32[768,1024]{1,0:T(8,128)} %copy.41), kind=kLoop, calls=%fused_computation.40 | loop fusion | flops 3932160 | bytes 15732736 | tf_op jit(solution)/shard_map/exp | solution.py:82
  124.3 4.2 slice.277
  128.5 4.2 slice.278
  132.6 7.7 %slice.276 = f32[384,1024]{1,0:T(8,128)} slice(f32[768,1024]{1,0:T(8,128)} %get-tuple-element.15), slice={[1:768:2], [0:1024:1]} | slice | bytes 3145728 | tf_op jit(solution)/shard_map/slice | solution.py:84
  140.3 7.6 %slice.280 = f32[384,1024]{1,0:T(8,128)} slice(f32[768,1024]{1,0:T(8,128)} %get-tuple-element.15), slice={[0:767:2], [0:1024:1]} | slice | bytes 3145728 | tf_op jit(solution)/shard_map/slice | solution.py:84
  147.9 5.5 fusion.43
  153.5 4.3 slice.283
  157.8 4.3 slice.284
  162.1 4.3 slice.282
  166.4 4.3 slice.286
  170.8 3.4 fusion.44
  237.4 4.4 slice.281
  241.8 4.4 slice.340
  247.6 4.4 slice.342
  252.0 7.7 %slice.275 = f32[383,1024]{1,0:T(8,128)} slice(f32[768,1024]{1,0:T(8,128)} %get-tuple-element.15), slice={[2:768:2], [0:1024:1]} | slice | bytes 3137536 | tf_op jit(solution)/shard_map/slice | solution.py:84
  275.3 9.7 %pad.84 = f32[768,1024]{1,0:T(8,128)} pad(f32[384,1024]{1,0:T(8,128)} %add.242, f32[]{:T(128)} %constant.11.clone.1), padding=1_0_1x0_0_0 | pad | bytes 4718596 | tf_op jit(solution)/shard_map/pad | solution.py:84
  287.8 5.6 pad.83
  293.4 9.1 %fusion.13 = f32[768,1024]{1,0:T(8,128)S(1)} fusion(f32[768,1024]{1,0:T(8,128)} %pad.83, f32[768,1024]{1,0:T(8,128)} %pad.84, bf16[2048,1024]{1,0:T(8,128)(2,1)} %all-gather.12.cloned.1.call-done, bf16[1,768,2048]{2,1,0:T(8,128)(2,1)} %all-gather.24.cloned.1.call-done, f32[2048]{0:T(1024)S(1)} %copy-done.29, f32[768]{0:T(1024)S(1)} %copy-done.26), kind=kOutput, calls=%fused_computation.26 | convolution fusion | flops 3236954112 | bytes 16788480 | tf_op jit(solution)/shard_map/dot_general | solution.py:32
  310.7 7.1 %convolution_convert_fusion = bf16[768,2048]{1,0:T(8,128)(2,1)} fusion(bf16[1024,2048]{1,0:T(8,128)(2,1)} %all-gather.14.cloned.1.call-done, f32[768,1024]{1,0:T(8,128)S(1)} %copy-done.7, f32[96,8,8,128]{3,2,1,0:T(8,128)S(1)} %bitcast.48, f32[1024]{0:T(1024)S(1)} %copy-done.31), kind=kOutput, calls=%fused_computation.15 | convolution fusion | flops 3225157632 | bytes 13635584 | tf_op jit(solution)/shard_map/dot_general | solution.py:90
  318.1 9.4 %reduce-scatter.3.cloned.1.call-done = bf16[768,1024]{1,0:T(8,128)(2,1)} async-done(((bf16[768,2048]{1,0:T(8,128)(2,1)}), bf16[768,1024]{1,0:T(8,128)(2,1)}) %reduce-scatter.3.cloned.1.call-update) | async-done | bytes 1572880 | tf_op jit(solution)/shard_map/reduce_scatter | solution.py:95
  327.6 3.2 fusion.16
  333.2 11.2 %all-gather.16.cloned.1.call-done = bf16[768,2048]{1,0:T(8,128)(2,1)} async-done(((bf16[768,1024]{1,0:T(8,128)(2,1)}), bf16[768,2048]{1,0:T(8,128)(2,1)}) %all-gather.16.cloned.1.call-update) | async-done | bytes 3145744 | tf_op jit(solution)/shard_map/all_gather | solution.py:99
  347.1 93.0 %all-gather.18.cloned.1.call-done = bf16[2048,1408]{1,0:T(8,128)(2,1)} async-done(((bf16[256,1408]{1,0:T(8,128)(2,1)}), bf16[2048,1408]{1,0:T(8,128)(2,1)}) %all-gather.18.cloned.1.call-update) | async-done | bytes 5767184 | tf_op jit(solution)/shard_map/all_gather | solution.py:104
  440.1 9.4 %fusion.7 = f32[768,1408]{1,0:T(8,128)} fusion(bf16[2048,1408]{1,0:T(8,128)(2,1)} %all-gather.18.cloned.1.call-done, bf16[768,2048]{1,0:T(8,128)(2,1)S(1)} %copy-done.5, f32[2048]{0:T(1024)S(1)} %copy-done.30, f32[768]{0:T(1024)S(1)} %add_rsqrt_fusion.1), kind=kOutput, calls=%fused_computation.20 | convolution fusion | flops 4437639168 | bytes 13249536 | tf_op jit(solution)/shard_map/dot_general | solution.py:31
  449.4 83.3 %all-gather.20.cloned.1.call-done = bf16[2048,1408]{1,0:T(8,128)(2,1)} async-done(((bf16[256,1408]{1,0:T(8,128)(2,1)}), bf16[2048,1408]{1,0:T(8,128)(2,1)}) %all-gather.20.cloned.1.call-update) | async-done | bytes 5767184 | tf_op jit(solution)/shard_map/all_gather | solution.py:105
  532.8 9.3 %fusion.6 = f32[768,1408]{1,0:T(8,128)} fusion(bf16[2048,1408]{1,0:T(8,128)(2,1)} %all-gather.20.cloned.1.call-done, bf16[768,2048]{1,0:T(8,128)(2,1)S(1)} %copy-done.5, f32[2048]{0:T(1024)S(1)} %copy-done.30, f32[768]{0:T(1024)S(1)} %add_rsqrt_fusion.1), kind=kOutput, calls=%fused_computation.18 | convolution fusion | flops 4437639168 | bytes 13249536 | tf_op jit(solution)/shard_map/dot_general | solution.py:32
  542.1 84.1 %all-gather.22.cloned.1.call-done = bf16[1408,2048]{1,0:T(8,128)(2,1)} async-done(((bf16[1408,256]{1,0:T(8,128)(2,1)}), bf16[1408,2048]{1,0:T(8,128)(2,1)}) %all-gather.22.cloned.1.call-update) | async-done | bytes 5767184 | tf_op jit(solution)/shard_map/all_gather | solution.py:115
  626.2 18.5 %convolution_convert_fusion.1 = bf16[768,2048]{1,0:T(8,128)(2,1)} fusion(bf16[1408,2048]{1,0:T(8,128)(2,1)} %all-gather.22.cloned.1.call-done, f32[768,1408]{1,0:T(8,128)} %fusion.6, f32[768,1408]{1,0:T(8,128)} %fusion.7, f32[1408]{0:T(1024)S(1)} %get-tuple-element.9, f32[1408]{0:T(1024)S(1)} %get-tuple-element.10, f32[1408]{0:T(1024)S(1)} %get-tuple-element.8, ...), kind=kOutput, calls=%fused_computation.16 | convolution fusion | flops 4448059392 | bytes 17597440 | tf_op jit(solution)/shard_map/dot_general | solution.py:113
  644.7 9.3 %reduce-scatter.5.cloned.1.call-done = bf16[768,1024]{1,0:T(8,128)(2,1)} async-done(((bf16[768,2048]{1,0:T(8,128)(2,1)}), bf16[768,1024]{1,0:T(8,128)(2,1)}) %reduce-scatter.5.cloned.1.call-update) | async-done | bytes 1572880 | tf_op jit(solution)/shard_map/reduce_scatter | solution.py:118
  (197 shorter events, 116.2 us)
Async XLA Ops:
  6.5 101.7 %copy-start = (bf16[8,128,128]{2,1,0:T(8,128)(2,1)S(1)}, bf16[8,128,128]{2,1,0:T(8,128)(2,1)}, u32[]{:S(2)}) copy-start(bf16[8,128,128]{2,1,0:T(8,128)(2,1)} %param.21) | copy-start | bytes 786436
  6.5 93.4 %copy-start.28 = (f32[2048]{0:T(1024)S(1)}, f32[2048]{0:T(1024)}, u32[]{:S(2)}) copy-start(f32[2048]{0:T(1024)} %param.17) | copy-start | bytes 24580
  6.5 17.2 %all-gather.24.cloned.1.call-start = ((), (), s32[]{:S(2)}) async-start(), calls=%async_computation.11 | async-start | bytes 4718592 | tf_op jit(solution)/shard_map/all_gather | solution.py:56
  7.3 92.6 %all-gather.10.cloned.1.call-start = ((), (), s32[]{:S(2)}) async-start(), calls=%async_computation.2 | async-start | bytes 4718592 | tf_op jit(solution)/shard_map/all_gather | solution.py:61
  8.0 285.4 %all-gather.12.cloned.1.call-start = ((), (), s32[]{:S(2)}) async-start(), calls=%async_computation.3 | async-start | bytes 4718592 | tf_op jit(solution)/shard_map/all_gather | solution.py:62
  8.8 300.0 %all-gather.14.cloned.1.call-start = ((), (), s32[]{:S(2)}) async-start(), calls=%async_computation.4 | async-start | bytes 4718592 | tf_op jit(solution)/shard_map/all_gather | solution.py:92
  9.3 318.2 %reduce-scatter.3.cloned.1.call-start = ((), (), s32[]{:S(2)}) async-start(), calls=%async_computation.5 | async-start | bytes 4718592 | tf_op jit(solution)/shard_map/reduce_scatter | solution.py:95
  23.8 76.1 %copy-start.4 = (bf16[1,768,2048]{2,1,0:T(8,128)(2,1)S(1)}, bf16[1,768,2048]{2,1,0:T(8,128)(2,1)}, u32[]{:S(2)}) copy-start(bf16[1,768,2048]{2,1,0:T(8,128)(2,1)} %all-gather.24.cloned.1.call-done) | copy-start | bytes 9437188
  26.5 78.7 %copy-start.25 = (f32[768]{0:T(1024)}, f32[768]{0:T(1024)S(1)}, u32[]{:S(2)}) copy-start(f32[768]{0:T(1024)S(1)} %add_rsqrt_fusion.2) | copy-start | bytes 9220
  247.6 12.7 %copy-start.12 = (f32[3,1024]{1,0:T(4,128)S(1)}, f32[3,1024]{1,0:T(4,128)}, u32[]{:S(2)}) copy-start(f32[3,1024]{1,0:T(4,128)} %slice.320) | copy-start | bytes 36868
  247.6 12.7 %copy-start.13 = (f32[3,1024]{1,0:T(4,128)S(1)}, f32[3,1024]{1,0:T(4,128)}, u32[]{:S(2)}) copy-start(f32[3,1024]{1,0:T(4,128)} %slice.318) | copy-start | bytes 36868
  247.6 12.7 %copy-start.14 = (f32[3,1024]{1,0:T(4,128)S(1)}, f32[3,1024]{1,0:T(4,128)}, u32[]{:S(2)}) copy-start(f32[3,1024]{1,0:T(4,128)} %slice.322) | copy-start | bytes 36868
  247.6 12.8 %copy-start.15 = (f32[2,1024]{1,0:T(2,128)S(1)}, f32[2,1024]{1,0:T(2,128)}, u32[]{:S(2)}) copy-start(f32[2,1024]{1,0:T(2,128)} %slice.317) | copy-start | bytes 24580
  247.6 12.8 %copy-start.16 = (f32[2,1024]{1,0:T(2,128)S(1)}, f32[2,1024]{1,0:T(2,128)}, u32[]{:S(2)}) copy-start(f32[2,1024]{1,0:T(2,128)} %slice.328) | copy-start | bytes 24580
  247.6 15.2 %copy-start.11 = (f32[11,1024]{1,0:T(8,128)S(1)}, f32[11,1024]{1,0:T(8,128)}, u32[]{:S(2)}) copy-start(f32[11,1024]{1,0:T(8,128)} %slice.332) | copy-start | bytes 135172
  260.3 6.0 copy-start.20
  266.6 4.3 copy-start.8
  287.7 5.7 copy-start.26
  287.7 5.7 copy-start.29
  304.9 5.7 copy-start.31
  317.8 9.8 %copy-start.3 = (bf16[1,768,1024]{2,1,0:T(8,128)(2,1)S(1)}, bf16[1,768,1024]{2,1,0:T(8,128)(2,1)}, u32[]{:S(2)}) copy-start(bf16[1,768,1024]{2,1,0:T(8,128)(2,1)} %param.16) | copy-start | bytes 4718596
  317.8 15.3 %copy-start.22 = (f32[3,1408]{1,0:T(4,128)S(1)}, f32[3,1408]{1,0:T(4,128)}, u32[]{:S(2)}) copy-start(f32[3,1408]{1,0:T(4,128)} %param.30) | copy-start | bytes 50692
  317.8 15.3 %copy-start.23 = (f32[3,1408]{1,0:T(4,128)S(1)}, f32[3,1408]{1,0:T(4,128)}, u32[]{:S(2)}) copy-start(f32[3,1408]{1,0:T(4,128)} %param.29) | copy-start | bytes 50692
  317.8 26.5 %all-gather.16.cloned.1.call-start = ((), (), s32[]{:S(2)}) async-start(), calls=%async_computation.6 | async-start | bytes 4718592 | tf_op jit(solution)/shard_map/all_gather | solution.py:99
  330.8 109.3 %copy-start.30 = (f32[2048]{0:T(1024)S(1)}, f32[2048]{0:T(1024)}, u32[]{:S(2)}) copy-start(f32[2048]{0:T(1024)} %param.26) | copy-start | bytes 24580
  330.8 109.3 %all-gather.18.cloned.1.call-start = ((), (), s32[]{:S(2)}) async-start(), calls=%async_computation.7 | async-start | bytes 6488064 | tf_op jit(solution)/shard_map/all_gather | solution.py:104
  331.6 201.2 %all-gather.20.cloned.1.call-start = ((), (), s32[]{:S(2)}) async-start(), calls=%async_computation.8 | async-start | bytes 6488064 | tf_op jit(solution)/shard_map/all_gather | solution.py:105
  332.3 293.9 %all-gather.22.cloned.1.call-start = ((), (), s32[]{:S(2)}) async-start(), calls=%async_computation.9 | async-start | bytes 6488064 | tf_op jit(solution)/shard_map/all_gather | solution.py:115
  333.0 320.9 %reduce-scatter.5.cloned.1.call-start = ((), (), s32[]{:S(2)}) async-start(), calls=%async_computation.10 | async-start | bytes 4718592 | tf_op jit(solution)/shard_map/reduce_scatter | solution.py:118
  344.4 95.7 %copy-start.5 = (bf16[768,2048]{1,0:T(8,128)(2,1)S(1)}, bf16[768,2048]{1,0:T(8,128)(2,1)}, u32[]{:S(2)}) copy-start(bf16[768,2048]{1,0:T(8,128)(2,1)} %all-gather.16.cloned.1.call-done) | copy-start | bytes 9437188
  644.7 9.3 %copy-start.2 = (bf16[768,1024]{1,0:T(8,128)(2,1)S(1)}, bf16[768,1024]{1,0:T(8,128)(2,1)}, u32[]{:S(2)}) copy-start(bf16[768,1024]{1,0:T(8,128)(2,1)} %fusion.16) | copy-start | bytes 4718596
  644.7 12.6 %copy-start.1 = (bf16[8,128,128]{2,1,0:T(8,128)(2,1)S(1)}, bf16[8,128,128]{2,1,0:T(8,128)(2,1)}, u32[]{:S(2)}) copy-start(bf16[8,128,128]{2,1,0:T(8,128)(2,1)} %param.21) | copy-start | bytes 786436
  (10 other events, 24.8 us)
Sparse Core Ops, SparseCore 0:
  8.9 14.8 all-gather.23
  25.9 73.9 all-gather.9
  102.0 71.3 all-gather.11
  175.3 73.1 all-gather.13
  317.9 9.5 reduce-scatter.2
  330.9 13.3 all-gather.15
  346.5 93.4 all-gather.17
  442.2 90.4 all-gather.19
  534.8 91.3 all-gather.21
  644.8 9.1 reduce-scatter.4
where the time goes:
time: 667 us; the launch traced here: 664 us
  waiting for transfers between devices  383 us (57%)
  local copies, waits for them, and re-layouts  149 us (22%)
  matrix products  62.3 us (9%)
  other arithmetic  55.8 us (8%)
  between operations  14.1 us (2%)
    slice x56, local copies, waits for them, and re-layouts, local(): _, states = lax.associative_scan(chain_combine, (decay, driven), axis=0)  118 us
    all_gather x1, waiting for transfers between devices, local(): lax.all_gather(gate_weight, 'fs', axis=0, tiled=True)  93 us
    all_gather x1, waiting for transfers between devices, local(): lax.all_gather(down_weight, 'fs', axis=1, tiled=True)  84.1 us
    all_gather x1, waiting for transfers between devices, local(): lax.all_gather(up_weight, 'fs', axis=0, tiled=True)  83.3 us
    all_gather x1, waiting for transfers between devices, local(): lax.all_gather(lin_weight, 'fs', axis=0, tiled=True)  73.4 us
    pad x17, local copies, waits for them, and re-layouts, local(): _, states = lax.associative_scan(chain_combine, (decay, driven), axis=0)  19.4 us
    dot_general x1, matrix products, local(): jnp.dot(hidden, lax.all_gather(down_weight, 'fs', axis=1, tiled=True), pr...  18.5 us
    dot_general x2, matrix products, pair_folder(): jnp.dot(source, pieces[1], preferred_element_type=jnp.float32)  18.5 us
  transfers between devices with their start and end apart: 10, of which 8 were waited for; matrix products, arithmetic and copies ran while one was open for 35% of the time, Pallas kernels for 0%

commit v1 on v0

--- a/solution.py
+++ b/solution.py
@@ -112,7 +112,7 @@
     hidden = (jax.nn.silu(gate_conv) * up_conv).astype(jnp.bfloat16)
     down_partial = jnp.dot(
         hidden,
-        lax.all_gather(down_weight, "fs", axis=1, tiled=True),
+        jnp.concatenate(lax.all_gather(down_weight, "fs"), axis=1),
         preferred_element_type=jnp.float32,
     )
     down_share = lax.psum_scatter(

time: 667 us -> 675 us (1.012)
  local copies, waits for them, and re-layouts: 149 us -> 157 us
    reshape x0 -> x1, local copies, waits for them, and re-layouts: none -> 8.29 us  [local(): jnp.concatenate(lax.all_gather(down_weight, 'fs'), axis=1)]
    all_gather x1, waiting for transfers between devices: 11.2 us -> 3.58 us  [local(): middle_full = lax.all_gather(middle_own, 'tp', axis=1, tiled=True)]
where the time goes in v1:
time: 675 us; the launch traced here: 671 us
  waiting for transfers between devices  381 us (56%)
  local copies, waits for them, and re-layouts  157 us (23%)
  matrix products  62.2 us (9%)
  other arithmetic  56 us (8%)
  between operations  14.1 us (2%)
    slice x56, local copies, waits for them, and re-layouts, local(): _, states = lax.associative_scan(chain_combine, (decay, driven), axis=0)  119 us
    all_gather x1, waiting for transfers between devices, local(): lax.all_gather(gate_weight, 'fs', axis=0, tiled=True)  93 us
    all_gather x1, waiting for transfers between devices, local(): lax.all_gather(down_weight, 'fs')  90.8 us
    all_gather x1, waiting for transfers between devices, local(): lax.all_gather(up_weight, 'fs', axis=0, tiled=True)  83.3 us
    all_gather x1, waiting for transfers between devices, local(): lax.all_gather(lin_weight, 'fs', axis=0, tiled=True)  73.4 us
    pad x17, local copies, waits for them, and re-layouts, local(): _, states = lax.associative_scan(chain_combine, (decay, driven), axis=0)  19.4 us
    dot_general x2, matrix products, pair_folder(): jnp.dot(source, pieces[1], preferred_element_type=jnp.float32)  18.5 us
    dot_general x1, matrix products, local(): jnp.dot(hidden, jnp.concatenate(lax.all_gather(down_weight, 'fs'), axis=1...  18.4 us
  transfers between devices with their start and end apart: 10, of which 8 were waited for; matrix products, arithmetic and copies ran while one was open for 35% of the time, Pallas kernels for 0%

profile of v1, /device:TPU:0, one launch (start us, length us, event | category | flops | bytes accessed | tf_op | source)
XLA Modules:
  0.0 671.5 jit_solution(1400090185979286221)
XLA Ops:
  9.4 14.3 %all-gather.23.cloned.1.call-done = bf16[1,768,2048]{2,1,0:T(8,128)(2,1)} async-done(((bf16[1,768,1024]{2,1,0:T(8,128)(2,1)}), bf16[1,768,2048]{2,1,0:T(8,128)(2,1)}) %all-gather.23.cloned.1.call-update) | async-done | bytes 3145744 | tf_op jit(solution)/shard_map/all_gather | solution.py:56
  26.5 73.4 %all-gather.11.cloned.1.call-done = bf16[2048,1024]{1,0:T(8,128)(2,1)} async-done(((bf16[256,1024]{1,0:T(8,128)(2,1)}), bf16[2048,1024]{1,0:T(8,128)(2,1)}) %all-gather.11.cloned.1.call-update) | async-done | bytes 4194320 | tf_op jit(solution)/shard_map/all_gather | solution.py:61
  99.9 5.3 fusion.18
  116.6 7.7 %multiply_exponential_fusion = (f32[768,1024]{1,0:T(8,128)}, f32[768,1024]{1,0:T(8,128)S(1)}) fusion(f32[768,1024]{1,0:T(8,128)} %copy.55, f32[1024]{0:T(1024)S(1)} %fusion.40, f32[768,1024]{1,0:T(8,128)} %get-tuple-element.14, f32[768,1024]{1,0:T(8,128)} %copy.56), kind=kLoop, calls=%fused_computation.40 | loop fusion | flops 3932160 | bytes 15732736 | tf_op jit(solution)/shard_map/exp | solution.py:82
  124.4 4.2 slice.277
  128.6 4.2 slice.278
  132.8 7.7 %slice.276 = f32[384,1024]{1,0:T(8,128)} slice(f32[768,1024]{1,0:T(8,128)} %get-tuple-element.15), slice={[1:768:2], [0:1024:1]} | slice | bytes 3145728 | tf_op jit(solution)/shard_map/slice | solution.py:84
  140.4 7.6 %slice.280 = f32[384,1024]{1,0:T(8,128)} slice(f32[768,1024]{1,0:T(8,128)} %get-tuple-element.15), slice={[0:767:2], [0:1024:1]} | slice | bytes 3145728 | tf_op jit(solution)/shard_map/slice | solution.py:84
  148.1 5.5 fusion.43
  153.6 4.3 slice.283
  157.9 4.3 slice.284
  162.3 4.3 slice.282
  166.6 4.4 slice.286
  171.0 3.4 fusion.44
  238.0 4.4 slice.281
  242.4 4.4 slice.340
  248.2 4.4 slice.342
  252.6 7.8 %slice.275 = f32[383,1024]{1,0:T(8,128)} slice(f32[768,1024]{1,0:T(8,128)} %get-tuple-element.15), slice={[2:768:2], [0:1024:1]} | slice | bytes 3137536 | tf_op jit(solution)/shard_map/slice | solution.py:84
  276.0 9.6 %pad.84 = f32[768,1024]{1,0:T(8,128)} pad(f32[384,1024]{1,0:T(8,128)} %add.242, f32[]{:T(128)} %constant.11.clone.1), padding=1_0_1x0_0_0 | pad | bytes 4718596 | tf_op jit(solution)/shard_map/pad | solution.py:84
  288.4 5.7 pad.83
  294.1 9.1 %fusion.13 = f32[768,1024]{1,0:T(8,128)S(1)} fusion(f32[768,1024]{1,0:T(8,128)} %pad.83, f32[768,1024]{1,0:T(8,128)} %pad.84, bf16[2048,1024]{1,0:T(8,128)(2,1)} %all-gather.13.cloned.1.call-done, bf16[1,768,2048]{2,1,0:T(8,128)(2,1)} %all-gather.23.cloned.1.call-done, f32[2048]{0:T(1024)S(1)} %copy-done.29, f32[768]{0:T(1024)S(1)} %copy-done.26), kind=kOutput, calls=%fused_computation.26 | convolution fusion | flops 3236954112 | bytes 16788480 | tf_op jit(solution)/shard_map/dot_general | solution.py:32
  311.4 7.1 %convolution_convert_fusion = bf16[768,2048]{1,0:T(8,128)(2,1)} fusion(bf16[1024,2048]{1,0:T(8,128)(2,1)} %all-gather.15.cloned.1.call-done, f32[768,1024]{1,0:T(8,128)S(1)} %copy-done.7, f32[96,8,8,128]{3,2,1,0:T(8,128)S(1)} %bitcast.54, f32[1024]{0:T(1024)S(1)} %copy-done.31), kind=kOutput, calls=%fused_computation.15 | convolution fusion | flops 3225157632 | bytes 13635584 | tf_op jit(solution)/shard_map/dot_general | solution.py:90
  319.4 9.0 %reduce-scatter.3.cloned.1.call-done = bf16[768,1024]{1,0:T(8,128)(2,1)} async-done(((bf16[768,2048]{1,0:T(8,128)(2,1)}), bf16[768,1024]{1,0:T(8,128)(2,1)}) %reduce-scatter.3.cloned.1.call-update) | async-done | bytes 1572880 | tf_op jit(solution)/shard_map/reduce_scatter | solution.py:95
  333.3 90.8 %all-gather.25.cloned.1.call-done = bf16[11264,256]{1,0:T(8,128)(2,1)} async-done(((bf16[1408,256]{1,0:T(8,128)(2,1)}), bf16[11264,256]{1,0:T(8,128)(2,1)}) %all-gather.25.cloned.1.call-update) | async-done | bytes 5767184 | tf_op jit(solution)/shard_map/all_gather | solution.py:115
  424.0 8.3 %copy.52 = bf16[1408,8,256]{0,2,1:T(8,128)(2,1)} copy(bf16[1408,8,256]{2,0,1:T(8,128)(2,1)} %bitcast.52) | data formatting | bytes 11534336 | tf_op jit(solution)/shard_map/reshape | solution.py:115
  432.3 3.6 all-gather.17.cloned.1.call-done
  438.7 93.0 %all-gather.19.cloned.1.call-done = bf16[2048,1408]{1,0:T(8,128)(2,1)} async-done(((bf16[256,1408]{1,0:T(8,128)(2,1)}), bf16[2048,1408]{1,0:T(8,128)(2,1)}) %all-gather.19.cloned.1.call-update) | async-done | bytes 5767184 | tf_op jit(solution)/shard_map/all_gather | solution.py:104
  531.6 9.4 %fusion.7 = f32[768,1408]{1,0:T(8,128)} fusion(bf16[2048,1408]{1,0:T(8,128)(2,1)} %all-gather.19.cloned.1.call-done, bf16[768,2048]{1,0:T(8,128)(2,1)S(1)} %copy-done.5, f32[2048]{0:T(1024)S(1)} %copy-done.30, f32[768]{0:T(1024)S(1)} %add_rsqrt_fusion.1), kind=kOutput, calls=%fused_computation.20 | convolution fusion | flops 4437639168 | bytes 13249536 | tf_op jit(solution)/shard_map/dot_general | solution.py:31
  541.0 83.3 %all-gather.21.cloned.1.call-done = bf16[2048,1408]{1,0:T(8,128)(2,1)} async-done(((bf16[256,1408]{1,0:T(8,128)(2,1)}), bf16[2048,1408]{1,0:T(8,128)(2,1)}) %all-gather.21.cloned.1.call-update) | async-done | bytes 5767184 | tf_op jit(solution)/shard_map/all_gather | solution.py:105
  624.3 9.3 %fusion.6 = f32[768,1408]{1,0:T(8,128)} fusion(bf16[2048,1408]{1,0:T(8,128)(2,1)} %all-gather.21.cloned.1.call-done, bf16[768,2048]{1,0:T(8,128)(2,1)S(1)} %copy-done.5, f32[2048]{0:T(1024)S(1)} %copy-done.30, f32[768]{0:T(1024)S(1)} %add_rsqrt_fusion.1), kind=kOutput, calls=%fused_computation.18 | convolution fusion | flops 4437639168 | bytes 13249536 | tf_op jit(solution)/shard_map/dot_general | solution.py:32
  633.7 18.4 %convolution_convert_fusion.1 = bf16[768,2048]{1,0:T(8,128)(2,1)} fusion(bf16[1408,2048]{0,1:T(8,128)(2,1)} %bitcast.53, f32[768,1408]{1,0:T(8,128)} %fusion.6, f32[768,1408]{1,0:T(8,128)} %fusion.7, f32[1408]{0:T(1024)S(1)} %get-tuple-element.9, f32[1408]{0:T(1024)S(1)} %get-tuple-element.10, f32[1408]{0:T(1024)S(1)} %get-tuple-element.8, ...), kind=kOutput, calls=%fused_computation.16 | convolution fusion | flops 4448059392 | bytes 17597440 | tf_op jit(solution)/shard_map/dot_general | solution.py:113
  652.1 9.3 %reduce-scatter.5.cloned.1.call-done = bf16[768,1024]{1,0:T(8,128)(2,1)} async-done(((bf16[768,2048]{1,0:T(8,128)(2,1)}), bf16[768,1024]{1,0:T(8,128)(2,1)}) %reduce-scatter.5.cloned.1.call-update) | async-done | bytes 1572880 | tf_op jit(solution)/shard_map/reduce_scatter | solution.py:118
  (198 shorter events, 119.8 us)
Async XLA Ops:
  6.5 101.7 %copy-start = (bf16[8,128,128]{2,1,0:T(8,128)(2,1)S(1)}, bf16[8,128,128]{2,1,0:T(8,128)(2,1)}, u32[]{:S(2)}) copy-start(bf16[8,128,128]{2,1,0:T(8,128)(2,1)} %param.21) | copy-start | bytes 786436
  6.5 93.4 %copy-start.28 = (f32[2048]{0:T(1024)S(1)}, f32[2048]{0:T(1024)}, u32[]{:S(2)}) copy-start(f32[2048]{0:T(1024)} %param.17) | copy-start | bytes 24580
  6.5 17.2 %all-gather.23.cloned.1.call-start = ((), (), s32[]{:S(2)}) async-start(), calls=%async_computation.10 | async-start | bytes 4718592 | tf_op jit(solution)/shard_map/all_gather | solution.py:56
  7.3 92.6 %all-gather.11.cloned.1.call-start = ((), (), s32[]{:S(2)}) async-start(), calls=%async_computation.2 | async-start | bytes 4718592 | tf_op jit(solution)/shard_map/all_gather | solution.py:61
  8.0 286.1 %all-gather.13.cloned.1.call-start = ((), (), s32[]{:S(2)}) async-start(), calls=%async_computation.3 | async-start | bytes 4718592 | tf_op jit(solution)/shard_map/all_gather | solution.py:62
  8.8 300.8 %all-gather.15.cloned.1.call-start = ((), (), s32[]{:S(2)}) async-start(), calls=%async_computation.4 | async-start | bytes 4718592 | tf_op jit(solution)/shard_map/all_gather | solution.py:92
  9.3 319.0 %reduce-scatter.3.cloned.1.call-start = ((), (), s32[]{:S(2)}) async-start(), calls=%async_computation.5 | async-start | bytes 4718592 | tf_op jit(solution)/shard_map/reduce_scatter | solution.py:95
  23.8 76.1 %copy-start.4 = (bf16[1,768,2048]{2,1,0:T(8,128)(2,1)S(1)}, bf16[1,768,2048]{2,1,0:T(8,128)(2,1)}, u32[]{:S(2)}) copy-start(bf16[1,768,2048]{2,1,0:T(8,128)(2,1)} %all-gather.23.cloned.1.call-done) | copy-start | bytes 9437188
  26.5 78.7 %copy-start.25 = (f32[768]{0:T(1024)}, f32[768]{0:T(1024)S(1)}, u32[]{:S(2)}) copy-start(f32[768]{0:T(1024)S(1)} %add_rsqrt_fusion.2) | copy-start | bytes 9220
  248.2 12.8 %copy-start.12 = (f32[3,1024]{1,0:T(4,128)S(1)}, f32[3,1024]{1,0:T(4,128)}, u32[]{:S(2)}) copy-start(f32[3,1024]{1,0:T(4,128)} %slice.320) | copy-start | bytes 36868
  248.2 12.8 %copy-start.13 = (f32[3,1024]{1,0:T(4,128)S(1)}, f32[3,1024]{1,0:T(4,128)}, u32[]{:S(2)}) copy-start(f32[3,1024]{1,0:T(4,128)} %slice.318) | copy-start | bytes 36868
  248.2 12.8 %copy-start.14 = (f32[3,1024]{1,0:T(4,128)S(1)}, f32[3,1024]{1,0:T(4,128)}, u32[]{:S(2)}) copy-start(f32[3,1024]{1,0:T(4,128)} %slice.322) | copy-start | bytes 36868
  248.2 12.9 %copy-start.15 = (f32[2,1024]{1,0:T(2,128)S(1)}, f32[2,1024]{1,0:T(2,128)}, u32[]{:S(2)}) copy-start(f32[2,1024]{1,0:T(2,128)} %slice.317) | copy-start | bytes 24580
  248.2 12.9 %copy-start.16 = (f32[2,1024]{1,0:T(2,128)S(1)}, f32[2,1024]{1,0:T(2,128)}, u32[]{:S(2)}) copy-start(f32[2,1024]{1,0:T(2,128)} %slice.328) | copy-start | bytes 24580
  248.2 15.2 %copy-start.11 = (f32[11,1024]{1,0:T(8,128)S(1)}, f32[11,1024]{1,0:T(8,128)}, u32[]{:S(2)}) copy-start(f32[11,1024]{1,0:T(8,128)} %slice.332) | copy-start | bytes 135172
  260.9 6.0 copy-start.20
  267.3 4.4 copy-start.8
  288.4 5.7 copy-start.26
  288.4 5.7 copy-start.29
  305.7 5.7 copy-start.31
  318.5 9.9 %copy-start.3 = (bf16[1,768,1024]{2,1,0:T(8,128)(2,1)S(1)}, bf16[1,768,1024]{2,1,0:T(8,128)(2,1)}, u32[]{:S(2)}) copy-start(bf16[1,768,1024]{2,1,0:T(8,128)(2,1)} %param.16) | copy-start | bytes 4718596
  318.5 105.5 %all-gather.25.cloned.1.call-start = ((), (), s32[]{:S(2)}) async-start(), calls=%async_computation.11 | async-start | bytes 6488064 | tf_op jit(solution)/shard_map/all_gather | solution.py:115
  319.1 14.0 %copy-start.22 = (f32[3,1408]{1,0:T(4,128)S(1)}, f32[3,1408]{1,0:T(4,128)}, u32[]{:S(2)}) copy-start(f32[3,1408]{1,0:T(4,128)} %param.30) | copy-start | bytes 50692
  319.1 14.0 %copy-start.23 = (f32[3,1408]{1,0:T(4,128)S(1)}, f32[3,1408]{1,0:T(4,128)}, u32[]{:S(2)}) copy-start(f32[3,1408]{1,0:T(4,128)} %param.29) | copy-start | bytes 50692
  319.1 116.8 %all-gather.17.cloned.1.call-start = ((), (), s32[]{:S(2)}) async-start(), calls=%async_computation.6 | async-start | bytes 4718592 | tf_op jit(solution)/shard_map/all_gather | solution.py:99
  331.6 200.0 %all-gather.19.cloned.1.call-start = ((), (), s32[]{:S(2)}) async-start(), calls=%async_computation.7 | async-start | bytes 6488064 | tf_op jit(solution)/shard_map/all_gather | solution.py:104
  332.4 292.0 %all-gather.21.cloned.1.call-start = ((), (), s32[]{:S(2)}) async-start(), calls=%async_computation.8 | async-start | bytes 6488064 | tf_op jit(solution)/shard_map/all_gather | solution.py:105
  333.1 328.3 %reduce-scatter.5.cloned.1.call-start = ((), (), s32[]{:S(2)}) async-start(), calls=%async_computation.9 | async-start | bytes 4718592 | tf_op jit(solution)/shard_map/reduce_scatter | solution.py:118
  432.3 99.3 %copy-start.30 = (f32[2048]{0:T(1024)S(1)}, f32[2048]{0:T(1024)}, u32[]{:S(2)}) copy-start(f32[2048]{0:T(1024)} %param.26) | copy-start | bytes 24580
  435.9 95.7 %copy-start.5 = (bf16[768,2048]{1,0:T(8,128)(2,1)S(1)}, bf16[768,2048]{1,0:T(8,128)(2,1)}, u32[]{:S(2)}) copy-start(bf16[768,2048]{1,0:T(8,128)(2,1)} %all-gather.17.cloned.1.call-done) | copy-start | bytes 9437188
  652.1 9.3 %copy-start.2 = (bf16[768,1024]{1,0:T(8,128)(2,1)S(1)}, bf16[768,1024]{1,0:T(8,128)(2,1)}, u32[]{:S(2)}) copy-start(bf16[768,1024]{1,0:T(8,128)(2,1)} %fusion.16) | copy-start | bytes 4718596
  652.1 12.5 %copy-start.1 = (bf16[8,128,128]{2,1,0:T(8,128)(2,1)S(1)}, bf16[8,128,128]{2,1,0:T(8,128)(2,1)}, u32[]{:S(2)}) copy-start(bf16[8,128,128]{2,1,0:T(8,128)(2,1)} %param.21) | copy-start | bytes 786436
  (10 other events, 24.9 us)
Sparse Core Ops, SparseCore 0:
  8.9 14.8 all-gather.22
  25.9 73.9 all-gather.10
  102.0 71.3 all-gather.12
  175.3 73.1 all-gather.14
  318.7 9.6 reduce-scatter.2
  330.4 93.5 all-gather.24
  425.6 10.2 all-gather.16
  438.1 93.4 all-gather.18
  533.8 90.4 all-gather.20
  652.2 9.1 reduce-scatter.4
